TPU v7x, 512 devices: a whole 4x4x16 slice. The times are simulated.
512 devices in a mesh: sp: 32 (over z, core), tp: 16 (over y, x).
Axes of the slice: x: 4, y: 4, z: 16, core: 2. Of those that a mesh axis runs over, the one named last changes fastest.
Arguments:
- queries: bfloat16 [16384, 1024], P('sp', 'tp'), may hold values from -20 to 20
- key_vectors: bfloat16 [16384, 1024], P('sp', 'tp'), may hold values from -20 to 20
- value_vectors: bfloat16 [16384, 1024], P('sp', 'tp'), may hold values from -6 to 6
- log_gate_sums: float32 [16384, 16], P('sp', 'tp'), may hold values from -2343 to 0, as said below
- residual: bfloat16 [16384, 2048], P('sp', 'tp'), may hold values from -24 to 24
- out_weight: bfloat16 [1024, 2048], P(None, 'tp'), may hold values from -0.75 to 0.75
- norm_gain: bfloat16 [2048], replicated, may hold values from 0.099609375 to 1.8984375
- routes: int32 [16384, 2], P('sp'), may hold values from 0 to 127, all different within a row; in each aligned block of 512 rows (0 to 511, 512 to 1023, ...) at most 10 rows name the same one
- route_weight: float32 [16384, 2], P('sp'), may hold values from 0.5 to 1.5
- expert_gate: bfloat16 [128, 2048, 512], P('sp', None, 'tp'), may hold values from -0.125 to 0.125
- expert_up: bfloat16 [128, 2048, 512], P('sp', None, 'tp'), may hold values from -0.125 to 0.125
- expert_down: bfloat16 [128, 512, 2048], P('sp', None, 'tp'), may hold values from -0.25 to 0.25
- shared_gate: bfloat16 [2048, 512], P(None, 'tp'), may hold values from -0.125 to 0.125
- shared_up: bfloat16 [2048, 512], P(None, 'tp'), may hold values from -0.125 to 0.125
- shared_down: bfloat16 [512, 2048], P(None, 'tp'), may hold values from -0.25 to 0.25
Outputs:
- layer_out: bfloat16 [16384, 2048], P('sp', 'tp')
Inputs may be any that keep to these rules, and one draw needn't show every extreme that they name: `log_gate_sums`: for each head the values do not rise along the positions. `routes`: each row names 2 different experts; among the rows of one index of sp no expert is named by more than 10 rows, a bound that some block reaches.
All inputs are finite; a program needn't handle non-finite values.
Results may differ from a plain program's by a relative error of at most 0.014.
Values may be sent and summed in bfloat16 or wider, within the bound.
No kernel may reach another device: no remote copies, remote signals or barrier semaphores. Data moves between devices by JAX's collectives and lax.ppermute only.
A program may use at most 64 MiB of HBM per device.

v0:
```python
import math
import jax
import jax.numpy as jnp
from jax import lax
from jax.sharding import PartitionSpec as P

HDIM = 64
EPSILON = 1e-06


def in_one_piece(arrays, axis, dim, along):
    both = jnp.concatenate(arrays, axis=along)
    filled, at, done = (lax.all_gather(both, axis, axis=dim, tiled=True), 0, [])
    for a in arrays:
        done.append(lax.slice_in_dim(filled, at, at + a.shape[along], axis=along))
        at += a.shape[along]
    return tuple(done)


def joined_along(tiles, dim):
    lengths = list(tiles.shape[1:])
    lengths[dim] *= tiles.shape[0]
    return jnp.moveaxis(tiles, 0, dim).reshape(lengths)


def sent_to_all(array, axis):
    copies = jnp.broadcast_to(array, (lax.axis_size(axis), *array.shape))
    return lax.all_to_all(copies, axis, split_axis=0, concat_axis=0, tiled=True)


def gather_directly(array, axis, dim):
    return joined_along(sent_to_all(array, axis), dim)


def over_copies(array, axis):
    everything = sent_to_all(array, axis)
    return jnp.sum(everything, axis=0)


def silu_gate(gate_part, up_part):
    return jax.nn.silu(gate_part) * up_part


def slot_targets(routes, experts_all, capacity):
    flat_routes = routes.reshape(-1)
    onehot = (flat_routes[:, None] == jnp.arange(experts_all, dtype=jnp.int32)[None, :]).astype(
        jnp.int32
    )
    before = jnp.cumsum(onehot, axis=0) - onehot
    return flat_routes * capacity + jnp.sum(before * onehot, axis=1)


def keep_state(fold_state):
    return fold_state


def shards(
    queries,
    key_vectors,
    value_vectors,
    log_gate_sums,
    residual,
    out_weight,
    norm_gain,
    routes,
    route_weight,
    expert_gate,
    expert_up,
    expert_down,
    shared_gate,
    shared_up,
    shared_down,
):
    tok_dev = queries.shape[0]
    head_dim = HDIM
    local_heads = log_gate_sums.shape[1]
    local_width = residual.shape[1]
    model_width = norm_gain.shape[0]
    score_scale = head_dim ** (-0.5)
    seq_first = lax.axis_index("sp") * tok_dev
    query_heads = queries.reshape(tok_dev, local_heads, head_dim)
    query_pos = seq_first + jnp.arange(tok_dev, dtype=jnp.int32)
    own_gates = log_gate_sums.T
    all_gates = lax.all_gather(log_gate_sums, "sp", axis=0, tiled=True)
    initial = (
        jnp.full((local_heads, tok_dev), -1e30, jnp.float32),
        jnp.zeros((local_heads, tok_dev), jnp.float32),
        jnp.zeros((local_heads, tok_dev, head_dim), jnp.float32),
    )
    key_heads = key_vectors.reshape(tok_dev, local_heads, head_dim)
    value_heads = value_vectors.reshape(tok_dev, local_heads, head_dim)
    key_part, value_part = in_one_piece((key_heads, value_heads), "sp", 0, 1)
    part_rows = key_part.shape[0]
    block_size = math.gcd(part_rows, 512)
    key_blocks = key_part.reshape(part_rows // block_size, block_size, local_heads, head_dim)
    value_blocks = value_part.reshape(part_rows // block_size, block_size, local_heads, head_dim)

    def one_block(fold_state, inputs):
        key_block, value_block, block_number = inputs
        block_first = block_number * block_size

        def compute(old_state):
            running_max, weight_total, summed = old_state
            gate_block = lax.dynamic_slice_in_dim(all_gates, block_first, block_size, 0).T
            scores = (
                jnp.einsum(
                    "qhd,khd->hqk", query_heads, key_block, preferred_element_type=jnp.float32
                )
                * score_scale
            )
            scores = scores + own_gates[:, :, None] - gate_block[:, None, :]
            key_pos = block_first + jnp.arange(block_size, dtype=jnp.int32)
            allowed = (key_pos[None, :] <= query_pos[:, None])[None]
            newmax = jnp.maximum(running_max, jnp.max(jnp.where(allowed, scores, -jnp.inf), axis=2))
            factor = jnp.exp(running_max - newmax)
            weight = jnp.where(allowed, jnp.exp(scores - newmax[:, :, None]), 0.0)
            weight_total = weight_total * factor + jnp.sum(weight, axis=2)
            summed = summed * factor[:, :, None] + jnp.einsum(
                "hqk,khd->hqd",
                weight.astype(jnp.bfloat16),
                value_block,
                preferred_element_type=jnp.float32,
            )
            return (newmax, weight_total, summed)

        useful = block_first <= seq_first + tok_dev - 1
        return (lax.cond(useful, compute, keep_state, fold_state), None)

    numbers = jnp.arange(part_rows // block_size, dtype=jnp.int32)
    result_state, _ = lax.scan(one_block, initial, (key_blocks, value_blocks, numbers))
    running_max, weight_total, summed = result_state
    attended = (summed / weight_total[:, :, None]).astype(jnp.bfloat16)
    attended = attended.transpose(1, 0, 2).reshape(tok_dev, local_heads * head_dim)
    weight_rows = out_weight
    projected = jnp.dot(
        gather_directly(attended, "tp", 1), weight_rows, preferred_element_type=jnp.float32
    )
    mid = (residual.astype(jnp.float32) + projected).astype(jnp.bfloat16)
    mid_wide = mid.astype(jnp.float32)
    feature_first = lax.axis_index("tp") * local_width
    squares = over_copies(jnp.sum(mid_wide * mid_wide, axis=1), "tp")
    inverse = lax.rsqrt(squares / model_width + EPSILON)
    own_gain = lax.dynamic_slice_in_dim(norm_gain, feature_first, local_width, 0).astype(
        jnp.float32
    )
    normed_own = (mid_wide * inverse[:, None] * own_gain[None, :]).astype(jnp.bfloat16)
    normed = gather_directly(normed_own, "tp", 1)
    shared_mid = silu_gate(
        jnp.dot(normed, shared_gate, preferred_element_type=jnp.float32),
        jnp.dot(normed, shared_up, preferred_element_type=jnp.float32),
    ).astype(jnp.bfloat16)
    weight_rows = shared_down
    shared_out = jnp.dot(
        lax.all_gather(shared_mid, "tp", axis=1, tiled=True),
        weight_rows,
        preferred_element_type=jnp.float32,
    )
    exp_dev = expert_gate.shape[0]
    sp_count = lax.axis_size("sp")
    experts_all = exp_dev * sp_count
    top_count = routes.shape[1]
    capacity = 5 * tok_dev * top_count // (4 * experts_all)
    targets = slot_targets(routes, experts_all, capacity)
    owners = (
        jnp.full((experts_all * capacity,), tok_dev, jnp.int32)
        .at[targets]
        .set(jnp.arange(tok_dev * top_count, dtype=jnp.int32) // top_count)
    )
    padded = jnp.concatenate(
        [normed_own, jnp.zeros((1, normed_own.shape[1]), jnp.bfloat16)], axis=0
    )
    outgoing = padded[owners].reshape(sp_count, exp_dev, capacity, normed_own.shape[1])
    rows_all = lax.all_gather(
        lax.all_to_all(outgoing, "sp", split_axis=0, concat_axis=0, tiled=True),
        "tp",
        axis=3,
        tiled=True,
    )
    gate_part = jnp.einsum(
        "secd,edf->secf", rows_all, expert_gate, preferred_element_type=jnp.float32
    )
    up_part = jnp.einsum("secd,edf->secf", rows_all, expert_up, preferred_element_type=jnp.float32)
    hidden = silu_gate(gate_part, up_part).astype(jnp.bfloat16)
    hidden_all = gather_directly(hidden, "tp", 3)
    produced = jnp.einsum(
        "secf,efd->secd", hidden_all, expert_down, preferred_element_type=jnp.float32
    ).astype(jnp.bfloat16)
    returned = lax.all_to_all(produced, "sp", split_axis=0, concat_axis=0, tiled=True)
    returned_flat = returned.reshape(experts_all * capacity, local_width)
    picked = returned_flat[targets].astype(jnp.float32).reshape(tok_dev, top_count, local_width)
    routed = jnp.sum(picked * route_weight[:, :, None], axis=1)
    return (mid_wide + shared_out + routed).astype(jnp.bfloat16)


def solution(mesh):
    placed = (
        P("sp", "tp"),
        P("sp", "tp"),
        P("sp", "tp"),
        P("sp", "tp"),
        P("sp", "tp"),
        P(None, "tp"),
        P(),
        P("sp", None),
        P("sp", None),
        P("sp", None, "tp"),
        P("sp", None, "tp"),
        P("sp", None, "tp"),
        P(None, "tp"),
        P(None, "tp"),
        P(None, "tp"),
    )
    return jax.shard_map(
        shards, mesh=mesh, in_specs=placed, out_specs=P("sp", "tp"), check_vma=False
    )
```

profile of v0, /device:TPU:32, one launch (start us, length us, event | category | flops | bytes accessed | tf_op | source)
XLA Modules:
  0.0 489.6 jit_solution(2940403956012515692)
XLA Ops:
  6.5 1.6 pad_maximum_fusion
  8.2 0.8 copy.77
  9.9 34.3 %all_gather.13 = f32[16384,1]{0,1:T(1,128)S(1)} all-gather(f32[512,1]{0,1:T(1,128)S(1)} %copy-done.8), channel_id=1, replica_groups=mesh['sp'=32,'tp'=16] {'sp'}, dimensions={0}, use_global_device_ids=true | all-gather | bytes 67584 | tf_op jit(solution)/shard_map/all_gather | solution.py:84
  44.2 43.0 %all-gather.3.cloned.1.call-done = bf16[16384,2,64]{0,2,1:T(8,128)(2,1)} async-done(((bf16[512,2,64]{0,2,1:T(8,128)(2,1)}), bf16[16384,2,64]{0,2,1:T(8,128)(2,1)}) %all-gather.3.cloned.1.call-update) | async-done | bytes 4194320 | tf_op jit(solution)/shard_map/all_gather | solution.py:13
  87.1 2.6 fusion.45
  89.7 2.5 copy_bitcast_fusion
  92.2 49.8 %while.17 = (s32[]{:T(128)}, f32[1,512]{1,0:T(1,128)S(1)}, f32[1,512]{1,0:T(1,128)S(1)}, f32[1,512,64]{1,2,0:T(8,128)S(1)}, s32[32]{0:T(128)S(1)}, /*index=5*/s3...) while((s32[]{:T(128)}, f32[1,512]{1,0:T(1,128)S(1)}, ...), condition=%wide.region_5.6_spmd.clone, body=%wide.region_0.5_spmd.clone.sunk | while | flops 70846464 | bytes 3667313 | solution.py:130
  93.5 2.9 conditional.3
  93.6 1.3 fusion.6
  95.2 1.2 fusion.5
  97.7 2.9 conditional.3
  97.8 1.3 fusion.6
  99.3 1.2 fusion.5
  101.8 2.9 conditional.3
  101.9 1.3 fusion.6
  103.4 1.2 fusion.5
  142.1 1.1 broadcast_in_dim.50
  143.2 6.7 %all-to-all-start = ((bf16[16,512,64]{1,2,0:T(8,128)(2,1)}), bf16[16,512,64]{1,2,0:T(8,128)(2,1)S(1)}, u32[]{:S(2)}, u32[]{:S(2)}) async-start(bf16[16,512,64]{1,2,0:T(8,128)(2,1)} %broadcast_in_dim.50), calls=%async_computation | async-start | bytes 2097152 | tf_op jit(solution)/shard_map/all_to_all | solution.py:28
  150.7 4.3 scatter_custom_fusion
  155.0 11.7 %all-to-all-done = bf16[16,512,64]{1,2,0:T(8,128)(2,1)S(1)} async-done(((bf16[16,512,64]{1,2,0:T(8,128)(2,1)}), bf16[16,512,64]{1,2,0:T(8,128)(2,1)S(1)}, u32[]{:S(2)}, u32[]{:S(2)}) %all-to-all-start) | async-done | bytes 1048608 | tf_op jit(solution)/shard_map/all_to_all | solution.py:28
  167.3 0.6 broadcast_in_dim.51
  167.9 4.5 all-to-all-start.1
  172.4 0.8 dynamic-slice_convert_fusion
  173.2 6.8 %all-to-all-done.1 = f32[16,1,512]{2,1,0:T(1,128)S(1)} async-done(((f32[16,1,512]{2,1,0:T(1,128)}), f32[16,1,512]{2,1,0:T(1,128)S(1)}, u32[]{:S(2)}, u32[]{:S(2)}) %all-to-all-start.1) | async-done | bytes 32800 | tf_op jit(solution)/shard_map/all_to_all | solution.py:28
  180.2 2.8 gather_fusion
  183.3 107.7 %all_to_all.31 = bf16[32,4,10,128]{3,1,2,0:T(4,128)(2,1)S(1)} all-to-all(bf16[32,4,10,128]{3,1,2,0:T(4,128)(2,1)S(1)} %copy.81), channel_id=1, replica_groups=mesh['sp'=32,'tp'=16] {'sp'}, dimensions={0} | all-to-all | bytes 655360 | tf_op jit(solution)/shard_map/all_to_all | solution.py:174
  291.0 0.8 copy.82
  291.8 66.5 %all-gather.5.cloned.1.call-done = bf16[32,4,10,2048]{3,0,2,1:T(8,128)(2,1)} async-done(((bf16[32,4,10,128]{3,0,2,1:T(8,128)(2,1)}), bf16[32,4,10,2048]{3,0,2,1:T(8,128)(2,1)}) %all-gather.5.cloned.1.call-update) | async-done | bytes 5242896 | tf_op jit(solution)/shard_map/all_gather | solution.py:173
  358.3 4.1 convolution_bitcast_fusion.2
  362.5 1.5 fusion.23
  364.0 3.6 broadcast_bitcast_fusion
  367.6 8.3 %reshape.202 = bf16[16,2,20480]{2,1,0:T(2,128)(2,1)} reshape(bf16[16,4,10,32,32]{4,3,2,1,0:T(8,128)(2,1)} %broadcast_bitcast_fusion) | data formatting | bytes 2621440
  375.9 4.9 %all-to-all-start.4 = ((bf16[16,2,20480]{2,1,0:T(2,128)(2,1)}), bf16[16,2,20480]{2,1,0:T(2,128)(2,1)S(1)}, u32[]{:S(2)}, u32[]{:S(2)}) async-start(bf16[16,2,20480]{2,1,0:T(2,128)(2,1)} %reshape.202), calls=%async_computation.4 | async-start | bytes 2621440 | tf_op jit(solution)/shard_map/all_to_all | solution.py:28
  381.0 19.0 %all-to-all-done.4 = bf16[16,2,20480]{2,1,0:T(2,128)(2,1)S(1)} async-done(((bf16[16,2,20480]{2,1,0:T(2,128)(2,1)}), bf16[16,2,20480]{2,1,0:T(2,128)(2,1)S(1)}, u32[]{:S(2)}, u32[]{:S(2)}) %all-to-all-start.4) | async-done | bytes 1310752 | tf_op jit(solution)/shard_map/all_to_all | solution.py:28
  399.9 1.7 broadcast_in_dim.52
  401.7 3.9 all-to-all-start.2
  405.6 7.2 %reshape.203 = bf16[16,4,10,32,32]{4,3,2,1,0:T(8,128)(2,1)} reshape(bf16[16,2,20480]{2,1,0:T(2,128)(2,1)} %copy-done.1) | data formatting | bytes 2621440
  412.9 3.8 bitcast_bitcast_fusion
  416.7 8.4 %copy.83 = bf16[32,4,10,16,32]{4,3,0,2,1:T(8,128)(2,1)} copy(bf16[32,4,10,16,32]{4,0,2,1,3:T(8,128)(2,1)S(1)} %bitcast_bitcast_fusion) | data formatting | bytes 2621440 | tf_op jit(solution)/shard_map/transpose | solution.py:23
  425.0 8.0 %reshape.169 = bf16[32,4,10,512]{3,0,2,1:T(8,128)(2,1)} reshape(bf16[32,4,10,16,32]{4,3,0,2,1:T(8,128)(2,1)} %copy.83) | data formatting | bytes 2621440 | tf_op jit(solution)/shard_map/reshape | solution.py:23
  433.0 1.8 fusion.24
  434.9 1.0 copy.84
  435.8 12.8 %all-to-all-start.5 = ((bf16[32,4,10,128]{3,1,2,0:T(4,128)(2,1)}), bf16[32,4,10,128]{3,1,2,0:T(4,128)(2,1)S(1)}, u32[]{:S(2)}, u32[]{:S(2)}) async-start(bf16[32,4,10,128]{3,1,2,0:T(4,128)(2,1)} %copy.84), calls=%async_computation.5 | async-start | bytes 655360 | tf_op jit(solution)/shard_map/all_to_all | solution.py:188
  448.8 1.4 fusion.46
  450.7 24.7 %all_gather.14 = bf16[512,512]{0,1:T(8,128)(2,1)S(1)} all-gather(bf16[512,32]{0,1:T(8,128)(2,1)S(1)} %fusion.29), channel_id=1, replica_groups=mesh['sp'=32,'tp'=16] {'tp'}, dimensions={1}, use_global_device_ids=true | all-gather | bytes 557056 | tf_op jit(solution)/shard_map/all_gather | solution.py:154
  475.7 3.2 gather_fusion.1
  478.9 2.8 fusion.30
  481.7 1.0 fusion.26
  (178 shorter events, 24.0 us)
Async XLA Ops:
  6.5 426.5 %copy-start = (bf16[4,512,128]{2,1,0:T(8,128)(2,1)S(1)}, bf16[4,512,128]{2,1,0:T(8,128)(2,1)}, u32[]{:S(2)}) copy-start(bf16[4,512,128]{2,1,0:T(8,128)(2,1)} %param.30) | copy-start | bytes 1572868
  6.5 3.3 copy-start.8
  6.5 80.6 %all-gather.3.cloned.1.call-start = ((), (), s32[]{:S(2)}) async-start(), calls=%async_computation.6 | async-start | bytes 4325376 | tf_op jit(solution)/shard_map/all_gather | solution.py:13
  89.7 2.5 copy-start.12
  142.1 7.9 %copy-start.6 = (s32[512,2]{0,1:T(2,128)S(1)}, s32[512,2]{0,1:T(2,128)}, u32[]{:S(2)}) copy-start(s32[512,2]{0,1:T(2,128)} %param.26) | copy-start | bytes 12292
  142.1 24.6 %copy-start.2 = (bf16[1024,128]{1,0:T(8,128)(2,1)S(1)}, bf16[1024,128]{1,0:T(8,128)(2,1)}, u32[]{:S(2)}) copy-start(bf16[1024,128]{1,0:T(8,128)(2,1)} %param.24) | copy-start | bytes 786436
  142.1 24.6 %copy-start.5 = (bf16[512,128]{1,0:T(8,128)(2,1)S(1)}, bf16[512,128]{1,0:T(8,128)(2,1)}, u32[]{:S(2)}) copy-start(bf16[512,128]{1,0:T(8,128)(2,1)} %param.23) | copy-start | bytes 393220
  143.2 23.5 %all-to-all-start = ((bf16[16,512,64]{1,2,0:T(8,128)(2,1)}), bf16[16,512,64]{1,2,0:T(8,128)(2,1)S(1)}, u32[]{:S(2)}, u32[]{:S(2)}) async-start(bf16[16,512,64]{1,2,0:T(8,128)(2,1)} %broadcast_in_dim.50), calls=%async_computation | async-start | bytes 2097152 | tf_op jit(solution)/shard_map/all_to_all | solution.py:28
  167.9 12.1 %all-to-all-start.1 = ((f32[16,1,512]{2,1,0:T(1,128)}), f32[16,1,512]{2,1,0:T(1,128)S(1)}, u32[]{:S(2)}, u32[]{:S(2)}) async-start(f32[16,1,512]{2,1,0:T(1,128)} %broadcast_in_dim.51), calls=%async_computation.1 | async-start | bytes 65536 | tf_op jit(solution)/shard_map/all_to_all | solution.py:28
  172.4 185.9 %all-gather.5.cloned.1.call-start = ((), (), s32[]{:S(2)}) async-start(), calls=%async_computation.7 | async-start | bytes 5570560 | tf_op jit(solution)/shard_map/all_gather | solution.py:173
  183.0 175.3 %copy-start.10 = (bf16[4,2048,32]{1,2,0:T(8,128)(2,1)S(1)}, bf16[4,2048,32]{1,2,0:T(8,128)(2,1)}, u32[]{:S(2)}) copy-start(bf16[4,2048,32]{1,2,0:T(8,128)(2,1)} %param.28) | copy-start | bytes 1572868
  291.8 70.6 %copy-start.11 = (bf16[4,2048,32]{1,2,0:T(8,128)(2,1)S(1)}, bf16[4,2048,32]{1,2,0:T(8,128)(2,1)}, u32[]{:S(2)}) copy-start(bf16[4,2048,32]{1,2,0:T(8,128)(2,1)} %param.29) | copy-start | bytes 1572868
  358.3 4.2 copy-start.9
  375.9 24.1 %all-to-all-start.4 = ((bf16[16,2,20480]{2,1,0:T(2,128)(2,1)}), bf16[16,2,20480]{2,1,0:T(2,128)(2,1)S(1)}, u32[]{:S(2)}, u32[]{:S(2)}) async-start(bf16[16,2,20480]{2,1,0:T(2,128)(2,1)} %reshape.202), calls=%async_computation.4 | async-start | bytes 2621440 | tf_op jit(solution)/shard_map/all_to_all | solution.py:28
  399.9 1.8 copy-start.1
  401.7 34.1 %all-to-all-start.2 = ((bf16[16,512,128]{1,2,0:T(8,128)(2,1)}), bf16[16,512,128]{1,2,0:T(8,128)(2,1)S(1)}, u32[]{:S(2)}, u32[]{:S(2)}) async-start(bf16[16,512,128]{1,2,0:T(8,128)(2,1)} %broadcast_in_dim.52), calls=%async_computation.2 | async-start | bytes 4194304 | tf_op jit(solution)/shard_map/all_to_all | solution.py:28
  433.0 15.6 %copy-start.7 = (f32[512,2]{0,1:T(2,128)S(1)}, f32[512,2]{0,1:T(2,128)}, u32[]{:S(2)}) copy-start(f32[512,2]{0,1:T(2,128)} %param.27) | copy-start | bytes 12292
  435.8 39.5 %all-to-all-start.5 = ((bf16[32,4,10,128]{3,1,2,0:T(4,128)(2,1)}), bf16[32,4,10,128]{3,1,2,0:T(4,128)(2,1)S(1)}, u32[]{:S(2)}, u32[]{:S(2)}) async-start(bf16[32,4,10,128]{3,1,2,0:T(4,128)(2,1)} %copy.84), calls=%async_computation.5 | async-start | bytes 655360 | tf_op jit(solution)/shard_map/all_to_all | solution.py:188
  448.8 1.4 copy-start.3
  475.5 6.2 %copy-start.4 = (bf16[512,128]{1,0:T(8,128)(2,1)S(1)}, bf16[512,128]{1,0:T(8,128)(2,1)}, u32[]{:S(2)}) copy-start(bf16[512,128]{1,0:T(8,128)(2,1)} %param.33) | copy-start | bytes 393220
Sparse Core Ops, SparseCore 0:
  9.5 77.6 all-gather.2
  291.9 66.3 all-gather.4
where the time goes:
time: 494 us; the launch traced here: 490 us
  blocking collectives  167 us (34%)
  waiting for transfers between devices  147 us (30%)
  local copies, waits for them, and re-layouts  81.5 us (16%)
  starting transfers between devices  32.9 us (7%)
  loops' own time  22.5 us (5%)
  matrix products  18.3 us (4%)
  between operations  13.9 us (3%)
  other arithmetic  6.84 us (1%)
    all_to_all x1, blocking collectives, shards(): lax.all_to_all(outgoing, 'sp', split_axis=0, concat_axis=0, tiled=True)  108 us
    all_gather x1, waiting for transfers between devices, shards(): lax.all_gather(lax.all_to_all(outgoing, 'sp', split_axis=0, concat_axis=0...  66.5 us
    all_gather x1, waiting for transfers between devices, in_one_piece(): filled, at, done = (lax.all_gather(both, axis, axis=dim, tiled=True), 0, [])  43 us
    all_to_all x4, waiting for transfers between devices, sent_to_all(): return lax.all_to_all(copies, axis, split_axis=0, concat_axis=0, tiled=True)  37.5 us
    all_gather x1, blocking collectives, shards(): all_gates = lax.all_gather(log_gate_sums, 'sp', axis=0, tiled=True)  34.3 us
    all_gather x1, blocking collectives, shards(): lax.all_gather(shared_mid, 'tp', axis=1, tiled=True)  24.7 us
    unnamed x32, local copies, waits for them, and re-layouts  22.7 us
    another operation x1, loops' own time, shards(): lax.scan(one_block, initial, (key_blocks, value_blocks, numbers))  22.1 us
  transfers between devices with their start and end apart: 7, of which 5 were waited for; matrix products, arithmetic and copies ran while one was open for 8% of the time, Pallas kernels for 0%

commit v1 on v0

--- a/solution.py
+++ b/solution.py
@@ -151,7 +151,7 @@
     ).astype(jnp.bfloat16)
     weight_rows = shared_down
     shared_out = jnp.dot(
-        lax.all_gather(shared_mid, "tp", axis=1, tiled=True),
+        jnp.concatenate(lax.all_gather(shared_mid, "tp"), axis=1),
         weight_rows,
         preferred_element_type=jnp.float32,
     )

time: 494 us -> 494 us (level)
  no operation moved by 1% of the time
where the time goes in v1:
time: 494 us; the launch traced here: 490 us
  blocking collectives  167 us (34%)
  waiting for transfers between devices  147 us (30%)
  local copies, waits for them, and re-layouts  81.6 us (17%)
  starting transfers between devices  32.9 us (7%)
  loops' own time  22.5 us (5%)
  matrix products  18.3 us (4%)
  between operations  13.9 us (3%)
  other arithmetic  6.84 us (1%)
    all_to_all x1, blocking collectives, shards(): lax.all_to_all(outgoing, 'sp', split_axis=0, concat_axis=0, tiled=True)  108 us
    all_gather x1, waiting for transfers between devices, shards(): lax.all_gather(lax.all_to_all(outgoing, 'sp', split_axis=0, concat_axis=0...  66.5 us
    all_gather x1, waiting for transfers between devices, in_one_piece(): filled, at, done = (lax.all_gather(both, axis, axis=dim, tiled=True), 0, [])  43 us
    all_to_all x4, waiting for transfers between devices, sent_to_all(): return lax.all_to_all(copies, axis, split_axis=0, concat_axis=0, tiled=True)  37.5 us
    all_gather x1, blocking collectives, shards(): all_gates = lax.all_gather(log_gate_sums, 'sp', axis=0, tiled=True)  34.3 us
    all_gather x1, blocking collectives, shards(): lax.all_gather(shared_mid, 'tp')  24.7 us
    unnamed x32, local copies, waits for them, and re-layouts  22.7 us
    another operation x1, loops' own time, shards(): lax.scan(one_block, initial, (key_blocks, value_blocks, numbers))  22.1 us
  transfers between devices with their start and end apart: 7, of which 5 were waited for; matrix products, arithmetic and copies ran while one was open for 8% of the time, Pallas kernels for 0%

profile of v1, /device:TPU:32, one launch (start us, length us, event | category | flops | bytes accessed | tf_op | source)
XLA Modules:
  0.0 489.6 jit_solution(2269844680615917342)
XLA Ops:
  6.5 1.6 pad_maximum_fusion
  8.2 0.8 copy.82
  9.9 34.3 %all_gather.16 = f32[16384,1]{0,1:T(1,128)S(1)} all-gather(f32[512,1]{0,1:T(1,128)S(1)} %copy-done.8), channel_id=1, replica_groups=mesh['sp'=32,'tp'=16] {'sp'}, dimensions={0}, use_global_device_ids=true | all-gather | bytes 67584 | tf_op jit(solution)/shard_map/all_gather | solution.py:84
  44.2 43.0 %all-gather.4.cloned.1.call-done = bf16[16384,2,64]{0,2,1:T(8,128)(2,1)} async-done(((bf16[512,2,64]{0,2,1:T(8,128)(2,1)}), bf16[16384,2,64]{0,2,1:T(8,128)(2,1)}) %all-gather.4.cloned.1.call-update) | async-done | bytes 4194320 | tf_op jit(solution)/shard_map/all_gather | solution.py:13
  87.1 2.6 fusion.45
  89.7 2.5 copy_bitcast_fusion
  92.2 49.8 %while.17 = (s32[]{:T(128)}, f32[1,512]{1,0:T(1,128)S(1)}, f32[1,512]{1,0:T(1,128)S(1)}, f32[1,512,64]{1,2,0:T(8,128)S(1)}, s32[32]{0:T(128)S(1)}, /*index=5*/s3...) while((s32[]{:T(128)}, f32[1,512]{1,0:T(1,128)S(1)}, ...), condition=%wide.region_5.6_spmd.clone, body=%wide.region_0.5_spmd.clone.sunk | while | flops 70846464 | bytes 3667313 | solution.py:130
  93.5 2.9 conditional.3
  93.6 1.3 fusion.6
  95.2 1.2 fusion.5
  97.7 2.9 conditional.3
  97.8 1.3 fusion.6
  99.3 1.2 fusion.5
  101.8 2.9 conditional.3
  101.9 1.3 fusion.6
  103.4 1.2 fusion.5
  142.1 1.1 broadcast_in_dim.50
  143.2 6.7 %all-to-all-start = ((bf16[16,512,64]{1,2,0:T(8,128)(2,1)}), bf16[16,512,64]{1,2,0:T(8,128)(2,1)S(1)}, u32[]{:S(2)}, u32[]{:S(2)}) async-start(bf16[16,512,64]{1,2,0:T(8,128)(2,1)} %broadcast_in_dim.50), calls=%async_computation | async-start | bytes 2097152 | tf_op jit(solution)/shard_map/all_to_all | solution.py:28
  150.7 4.3 scatter_custom_fusion
  155.0 11.7 %all-to-all-done = bf16[16,512,64]{1,2,0:T(8,128)(2,1)S(1)} async-done(((bf16[16,512,64]{1,2,0:T(8,128)(2,1)}), bf16[16,512,64]{1,2,0:T(8,128)(2,1)S(1)}, u32[]{:S(2)}, u32[]{:S(2)}) %all-to-all-start) | async-done | bytes 1048608 | tf_op jit(solution)/shard_map/all_to_all | solution.py:28
  167.3 0.6 broadcast_in_dim.51
  167.9 4.5 all-to-all-start.1
  172.4 0.8 dynamic-slice_convert_fusion
  173.2 6.8 %all-to-all-done.1 = f32[16,1,512]{2,1,0:T(1,128)S(1)} async-done(((f32[16,1,512]{2,1,0:T(1,128)}), f32[16,1,512]{2,1,0:T(1,128)S(1)}, u32[]{:S(2)}, u32[]{:S(2)}) %all-to-all-start.1) | async-done | bytes 32800 | tf_op jit(solution)/shard_map/all_to_all | solution.py:28
  180.2 2.8 gather_fusion
  183.3 107.7 %all_to_all.31 = bf16[32,4,10,128]{3,1,2,0:T(4,128)(2,1)S(1)} all-to-all(bf16[32,4,10,128]{3,1,2,0:T(4,128)(2,1)S(1)} %copy.86), channel_id=1, replica_groups=mesh['sp'=32,'tp'=16] {'sp'}, dimensions={0} | all-to-all | bytes 655360 | tf_op jit(solution)/shard_map/all_to_all | solution.py:174
  291.0 0.8 copy.87
  291.8 66.5 %all-gather.6.cloned.1.call-done = bf16[32,4,10,2048]{3,0,2,1:T(8,128)(2,1)} async-done(((bf16[32,4,10,128]{3,0,2,1:T(8,128)(2,1)}), bf16[32,4,10,2048]{3,0,2,1:T(8,128)(2,1)}) %all-gather.6.cloned.1.call-update) | async-done | bytes 5242896 | tf_op jit(solution)/shard_map/all_gather | solution.py:173
  358.3 4.1 convolution_bitcast_fusion.2
  362.5 1.5 fusion.23
  364.0 3.6 broadcast_bitcast_fusion
  367.6 8.3 %reshape.211 = bf16[16,2,20480]{2,1,0:T(2,128)(2,1)} reshape(bf16[16,4,10,32,32]{4,3,2,1,0:T(8,128)(2,1)} %broadcast_bitcast_fusion) | data formatting | bytes 2621440
  375.9 4.9 %all-to-all-start.4 = ((bf16[16,2,20480]{2,1,0:T(2,128)(2,1)}), bf16[16,2,20480]{2,1,0:T(2,128)(2,1)S(1)}, u32[]{:S(2)}, u32[]{:S(2)}) async-start(bf16[16,2,20480]{2,1,0:T(2,128)(2,1)} %reshape.211), calls=%async_computation.4 | async-start | bytes 2621440 | tf_op jit(solution)/shard_map/all_to_all | solution.py:28
  381.0 19.0 %all-to-all-done.4 = bf16[16,2,20480]{2,1,0:T(2,128)(2,1)S(1)} async-done(((bf16[16,2,20480]{2,1,0:T(2,128)(2,1)}), bf16[16,2,20480]{2,1,0:T(2,128)(2,1)S(1)}, u32[]{:S(2)}, u32[]{:S(2)}) %all-to-all-start.4) | async-done | bytes 1310752 | tf_op jit(solution)/shard_map/all_to_all | solution.py:28
  399.9 1.7 broadcast_in_dim.52
  401.7 3.9 all-to-all-start.2
  405.6 7.2 %reshape.212 = bf16[16,4,10,32,32]{4,3,2,1,0:T(8,128)(2,1)} reshape(bf16[16,2,20480]{2,1,0:T(2,128)(2,1)} %copy-done.1) | data formatting | bytes 2621440
  412.9 3.8 bitcast_bitcast_fusion
  416.7 8.4 %copy.88 = bf16[32,4,10,16,32]{4,3,0,2,1:T(8,128)(2,1)} copy(bf16[32,4,10,16,32]{4,0,2,1,3:T(8,128)(2,1)S(1)} %bitcast_bitcast_fusion) | data formatting | bytes 2621440 | tf_op jit(solution)/shard_map/transpose | solution.py:23
  425.0 8.0 %reshape.177 = bf16[32,4,10,512]{3,0,2,1:T(8,128)(2,1)} reshape(bf16[32,4,10,16,32]{4,3,0,2,1:T(8,128)(2,1)} %copy.88) | data formatting | bytes 2621440 | tf_op jit(solution)/shard_map/reshape | solution.py:23
  433.0 1.8 fusion.24
  434.9 1.0 copy.89
  435.8 12.8 %all-to-all-start.5 = ((bf16[32,4,10,128]{3,1,2,0:T(4,128)(2,1)}), bf16[32,4,10,128]{3,1,2,0:T(4,128)(2,1)S(1)}, u32[]{:S(2)}, u32[]{:S(2)}) async-start(bf16[32,4,10,128]{3,1,2,0:T(4,128)(2,1)} %copy.89), calls=%async_computation.5 | async-start | bytes 655360 | tf_op jit(solution)/shard_map/all_to_all | solution.py:188
  448.8 1.4 fusion.46
  450.7 24.7 %all-gather = bf16[8192,32]{0,1:T(8,128)(2,1)S(1)} all-gather(bf16[512,32]{0,1:T(8,128)(2,1)S(1)} %fusion.29), channel_id=2, replica_groups=mesh['sp'=32,'tp'=16] {'tp'}, dimensions={0}, use_global_device_ids=true | all-gather | bytes 557056 | tf_op jit(solution)/shard_map/all_gather | solution.py:154
  475.7 3.2 gather_fusion.1
  479.0 2.8 fusion.30
  481.8 1.0 fusion.26
  (179 shorter events, 24.0 us)
Async XLA Ops:
  6.5 426.5 %copy-start = (bf16[4,512,128]{2,1,0:T(8,128)(2,1)S(1)}, bf16[4,512,128]{2,1,0:T(8,128)(2,1)}, u32[]{:S(2)}) copy-start(bf16[4,512,128]{2,1,0:T(8,128)(2,1)} %param.30) | copy-start | bytes 1572868
  6.5 3.3 copy-start.8
  6.5 80.6 %all-gather.4.cloned.1.call-start = ((), (), s32[]{:S(2)}) async-start(), calls=%async_computation.6 | async-start | bytes 4325376 | tf_op jit(solution)/shard_map/all_gather | solution.py:13
  89.7 2.5 copy-start.12
  142.1 7.9 %copy-start.6 = (s32[512,2]{0,1:T(2,128)S(1)}, s32[512,2]{0,1:T(2,128)}, u32[]{:S(2)}) copy-start(s32[512,2]{0,1:T(2,128)} %param.26) | copy-start | bytes 12292
  142.1 24.6 %copy-start.2 = (bf16[1024,128]{1,0:T(8,128)(2,1)S(1)}, bf16[1024,128]{1,0:T(8,128)(2,1)}, u32[]{:S(2)}) copy-start(bf16[1024,128]{1,0:T(8,128)(2,1)} %param.24) | copy-start | bytes 786436
  142.1 24.6 %copy-start.5 = (bf16[512,128]{1,0:T(8,128)(2,1)S(1)}, bf16[512,128]{1,0:T(8,128)(2,1)}, u32[]{:S(2)}) copy-start(bf16[512,128]{1,0:T(8,128)(2,1)} %param.23) | copy-start | bytes 393220
  143.2 23.5 %all-to-all-start = ((bf16[16,512,64]{1,2,0:T(8,128)(2,1)}), bf16[16,512,64]{1,2,0:T(8,128)(2,1)S(1)}, u32[]{:S(2)}, u32[]{:S(2)}) async-start(bf16[16,512,64]{1,2,0:T(8,128)(2,1)} %broadcast_in_dim.50), calls=%async_computation | async-start | bytes 2097152 | tf_op jit(solution)/shard_map/all_to_all | solution.py:28
  167.9 12.1 %all-to-all-start.1 = ((f32[16,1,512]{2,1,0:T(1,128)}), f32[16,1,512]{2,1,0:T(1,128)S(1)}, u32[]{:S(2)}, u32[]{:S(2)}) async-start(f32[16,1,512]{2,1,0:T(1,128)} %broadcast_in_dim.51), calls=%async_computation.1 | async-start | bytes 65536 | tf_op jit(solution)/shard_map/all_to_all | solution.py:28
  172.4 185.9 %all-gather.6.cloned.1.call-start = ((), (), s32[]{:S(2)}) async-start(), calls=%async_computation.7 | async-start | bytes 5570560 | tf_op jit(solution)/shard_map/all_gather | solution.py:173
  183.0 175.3 %copy-start.10 = (bf16[4,2048,32]{1,2,0:T(8,128)(2,1)S(1)}, bf16[4,2048,32]{1,2,0:T(8,128)(2,1)}, u32[]{:S(2)}) copy-start(bf16[4,2048,32]{1,2,0:T(8,128)(2,1)} %param.28) | copy-start | bytes 1572868
  291.8 70.6 %copy-start.11 = (bf16[4,2048,32]{1,2,0:T(8,128)(2,1)S(1)}, bf16[4,2048,32]{1,2,0:T(8,128)(2,1)}, u32[]{:S(2)}) copy-start(bf16[4,2048,32]{1,2,0:T(8,128)(2,1)} %param.29) | copy-start | bytes 1572868
  358.3 4.2 copy-start.9
  375.9 24.1 %all-to-all-start.4 = ((bf16[16,2,20480]{2,1,0:T(2,128)(2,1)}), bf16[16,2,20480]{2,1,0:T(2,128)(2,1)S(1)}, u32[]{:S(2)}, u32[]{:S(2)}) async-start(bf16[16,2,20480]{2,1,0:T(2,128)(2,1)} %reshape.211), calls=%async_computation.4 | async-start | bytes 2621440 | tf_op jit(solution)/shard_map/all_to_all | solution.py:28
  399.9 1.8 copy-start.1
  401.7 34.1 %all-to-all-start.2 = ((bf16[16,512,128]{1,2,0:T(8,128)(2,1)}), bf16[16,512,128]{1,2,0:T(8,128)(2,1)S(1)}, u32[]{:S(2)}, u32[]{:S(2)}) async-start(bf16[16,512,128]{1,2,0:T(8,128)(2,1)} %broadcast_in_dim.52), calls=%async_computation.2 | async-start | bytes 4194304 | tf_op jit(solution)/shard_map/all_to_all | solution.py:28
  433.0 15.6 %copy-start.7 = (f32[512,2]{0,1:T(2,128)S(1)}, f32[512,2]{0,1:T(2,128)}, u32[]{:S(2)}) copy-start(f32[512,2]{0,1:T(2,128)} %param.27) | copy-start | bytes 12292
  435.8 39.6 %all-to-all-start.5 = ((bf16[32,4,10,128]{3,1,2,0:T(4,128)(2,1)}), bf16[32,4,10,128]{3,1,2,0:T(4,128)(2,1)S(1)}, u32[]{:S(2)}, u32[]{:S(2)}) async-start(bf16[32,4,10,128]{3,1,2,0:T(4,128)(2,1)} %copy.89), calls=%async_computation.5 | async-start | bytes 655360 | tf_op jit(solution)/shard_map/all_to_all | solution.py:188
  448.8 1.4 copy-start.3
  475.6 6.2 %copy-start.4 = (bf16[512,128]{1,0:T(8,128)(2,1)S(1)}, bf16[512,128]{1,0:T(8,128)(2,1)}, u32[]{:S(2)}) copy-start(bf16[512,128]{1,0:T(8,128)(2,1)} %param.33) | copy-start | bytes 393220
Sparse Core Ops, SparseCore 0:
  9.5 77.6 all-gather.3
  291.9 66.3 all-gather.5
